TPU v7x, 32 devices: a whole 2x2x4 slice. The times are simulated.
32 devices in a mesh: grp: 2 (over y), st: 8 (over z, core), tp: 2 (over x).
Axes of the slice: x: 2, y: 2, z: 4, core: 2. Of those that a mesh axis runs over, the one named last changes fastest.
Arguments:
- tokens: bfloat16 [8192, 2048], P(('grp', 'st')), parts along dimension 0, may hold values from -6 to 6
- owners: int32 [128, 4], P(('grp', 'st')), parts along dimension 0, may hold values from 0 to 7, all different within a row; in each aligned block of 8 rows (0 to 7, 8 to 15, ...) at most 8 rows name the same one
- entries: int32 [128, 4], P(('grp', 'st')), parts along dimension 0, may hold values from 0 to 15
- store: bfloat16 [256, 64, 2048], P(('grp', 'st')), parts along dimension 0, may hold values from -600 to 600
- mixer_query_weight: bfloat16 [2048, 1024], P(None, 'tp'), may hold values from -0.125 to 0.125
- mixer_key_weight: bfloat16 [2048, 1024], P(None, 'tp'), may hold values from -0.125 to 0.125
- mixer_value_weight: bfloat16 [2048, 1024], P(None, 'tp'), may hold values from -0.125 to 0.125
- strength_weight: bfloat16 [2048, 8], P(None, 'tp'), may hold values from -0.125 to 0.125
- decay_weight: bfloat16 [2048, 8], P(None, 'tp'), may hold values from -0.125 to 0.125
- head_decay_rate: float32 [8], P('tp'), may hold values from 0.003 to 0.15
- extra_forgetting_exponent: float32 [8192, 8], P(('grp', 'st'), 'tp'), parts along dimension 0, may hold values from -0.7 to 0
- output_norm_gain: float32 [128], replicated, may hold values from 0.1 to 1.9
- retrieval_query_weight: bfloat16 [2048, 1024], P(None, 'tp'), may hold values from -0.125 to 0.125
- passage_key_weight: bfloat16 [2048, 1024], P(None, 'tp'), may hold values from -0.125 to 0.125
- passage_value_weight: bfloat16 [2048, 1024], P(None, 'tp'), may hold values from -0.125 to 0.125
- retrieval_gate_weight: bfloat16 [2048, 8], P(None, 'tp'), may hold values from -0.125 to 0.125
Outputs:
- mixed: bfloat16 [8192, 1024], P(('grp', 'st'), 'tp'), parts along dimension 0
There are 2 independent parts, one for each index of `grp`. A program takes and returns all parts, laid end to end along the dimension named above; an argument that names none is the same for every part. Nothing has to cross between parts.
Inputs may be any that keep to these rules, and one draw needn't show every extreme that they name: `owners`: each row names 4 different values; the rows of one device name no value more than 8 times, a bound that some device reaches; every value is named by some row.
All inputs are finite; a program needn't handle non-finite values.
Results may differ from a plain program's by a relative error of at most 0.015.
The roundings to bfloat16 on the way count: a program that leaves them out, or rounds other values in their place, can miss the bound.
Values may be sent and summed in bfloat16 or wider, within the bound.
A program may use at most 128 MiB of HBM per device.

v0:
```python
import functools

import jax
import jax.numpy as jnp
from jax import lax
from jax.experimental import pallas as pl
from jax.experimental.pallas import tpu as pltpu
from jax.sharding import PartitionSpec as P

BLOCK = 64
EPS = 1e-06
MISSING = -1e30
F32 = jnp.float32
BF16 = jnp.bfloat16
SPAN = 128


def dot_nn(left, right):
    return jnp.dot(left, right, preferred_element_type=F32)


def dot_nt(left, right):
    return lax.dot_general(left, right, (((1,), (1,)), ((), ())), preferred_element_type=F32)


def dot_tn(left, right):
    return lax.dot_general(left, right, (((0,), (0,)), ((), ())), preferred_element_type=F32)


def attend_unit(q_ref, named, me, sibling, kv_own, kv_sib, o_ref, stat_ref, passage_rows, head_dim):
    length, half = q_ref.shape
    heads = half // head_dim
    blocks = length // BLOCK
    scale = head_dim ** (-0.5)
    nothing = jnp.zeros((BLOCK, head_dim), BF16)

    def find(pairs, device):
        hit = jnp.int32(0)
        for owner, entry in pairs:
            hit = hit + (owner == device).astype(jnp.int32) * (entry + 1)
        found = jnp.minimum(hit, 1)
        return hit - found, (1 - found).astype(F32) * MISSING

    places, scores = [], []
    for block in range(blocks):
        pairs = named(block)
        row_own, bias_own = find(pairs, me)
        row_sib, bias_sib = find(pairs, sibling)
        places.append((row_own, bias_own, row_sib, bias_sib))
        query = q_ref[block * BLOCK : (block + 1) * BLOCK, :]
        spread = jnp.concatenate(
            [
                jnp.concatenate(
                    [
                        query[:, head * head_dim : (head + 1) * head_dim] if head == place else nothing
                        for place in range(heads)
                    ],
                    axis=1,
                )
                for head in range(heads)
            ],
            axis=0,
        )
        keys = jnp.concatenate(
            [
                kv_own[row_own, :, :half],
                kv_sib[row_sib, :, :half],
            ],
            axis=0,
        )
        scores.append(dot_nt(keys, spread))
    weights, stats = [], []
    for block in range(blocks):
        _, bias_own, _, bias_sib = places[block]
        raw = scores[block]
        own = raw[:passage_rows] * scale + bias_own
        sib = raw[passage_rows:] * scale + bias_sib
        peak = jnp.max(jnp.maximum(own, sib), axis=0, keepdims=True)
        e_own = jnp.exp(own - peak)
        e_sib = jnp.exp(sib - peak)
        total = jnp.sum(e_own + e_sib, axis=0, keepdims=True)
        inv = 1.0 / total
        weights.append(jnp.concatenate([e_own * inv, e_sib * inv], axis=0).astype(BF16))
        stats.append(peak + jnp.log(total))
    for block in range(blocks):
        row_own, _, row_sib, _ = places[block]
        values = jnp.concatenate(
            [
                kv_own[row_own, :, half:],
                kv_sib[row_sib, :, half:],
            ],
            axis=0,
        )
        result = dot_tn(weights[block], values)
        for head in range(heads):
            cols = slice(head * head_dim, (head + 1) * head_dim)
            o_ref[block * BLOCK : (block + 1) * BLOCK, cols] = result[
                head * BLOCK : (head + 1) * BLOCK, cols
            ].astype(BF16)
    rows = jnp.concatenate(stats, axis=0)
    spare = stat_ref.shape[1] - rows.shape[1]
    if spare:
        rows = jnp.concatenate([rows, jnp.zeros((blocks, spare), F32)], axis=1)
    stat_ref[...] = rows


def gate_rows(gates, extra_ref, rate_ref):
    heads, length = extra_ref.shape
    rows = jnp.transpose(gates)
    beta = jax.nn.sigmoid(rows[:heads])
    raw = rows[heads : 2 * heads]
    softplus = jnp.maximum(raw, 0.0) + jnp.log1p(jnp.exp(-jnp.abs(raw)))
    which = lax.broadcasted_iota(jnp.int32, (heads, length), 0)
    rate = jnp.zeros((heads, length), F32)
    for head in range(heads):
        rate = jnp.where(which == head, rate_ref[head], rate)
    decay = -rate * softplus + extra_ref[...]
    rgate = jax.nn.sigmoid(rows[2 * heads : 3 * heads])
    tri = jnp.where(
        lax.broadcasted_iota(jnp.int32, (SPAN, SPAN), 0)
        <= lax.broadcasted_iota(jnp.int32, (SPAN, SPAN), 1),
        1.0,
        0.0,
    ).astype(F32)
    pad = jnp.zeros((8 - heads, SPAN), F32)
    spans = []
    for span in range(length // SPAN):
        at = slice(span * SPAN, (span + 1) * SPAN)
        cum = jnp.dot(
            jnp.concatenate([decay[:, at], pad], axis=0),
            tri,
            precision=lax.Precision.HIGHEST,
            preferred_element_type=F32,
        )[:heads]
        ends = cum[:, SPAN - 1 : SPAN]
        grow = jnp.exp(cum)
        cols = jnp.transpose(jnp.concatenate([cum, beta[:, at], grow, rgate[:, at]], axis=0))
        spans.append((cum, beta[:, at], beta[:, at] * grow, jnp.exp(ends - cum), jnp.exp(ends), cols))
    return spans


def delta_body(spans, read, gain, heads, store):
    head_dim = gain.shape[1]
    count = len(spans)
    half = SPAN // 2
    row = lax.broadcasted_iota(jnp.int32, (SPAN, SPAN), 0)
    col = lax.broadcasted_iota(jnp.int32, (SPAN, SPAN), 1)
    lower = row >= col
    strict = row > col
    prow = lax.broadcasted_iota(jnp.int32, (half, SPAN), 0)
    plane = lax.broadcasted_iota(jnp.int32, (half, SPAN), 1)
    pcol = plane % half
    is_left = plane < half
    left = jnp.where(is_left, 1.0, 0.0).astype(BF16)
    right = jnp.where(is_left, 0.0, 1.0).astype(BF16)
    eye = jnp.where(prow == pcol, 1.0, 0.0).astype(F32)
    sizes = []
    size = 2
    while size < half:
        sizes.append(size)
        size *= 2

    def cut_of(size):
        return ((prow // (2 * size)) == (pcol // (2 * size))) & ((prow // size) != (pcol // size))

    first = jnp.where(cut_of(1), 1.0, 0.0).astype(F32)
    cuts = []
    for size in sizes:
        cut = jnp.where(cut_of(size), 1.0, 0.0).astype(BF16)
        cuts.append((cut * left, cut * right))
    units = [(head, span) for head in range(heads) for span in range(count)]
    kb, kt, grams, mixes = {}, {}, {}, {}
    for unit in units:
        k32 = read("k", *unit).astype(F32)
        kn = k32 * lax.rsqrt(jnp.sum(k32 * k32, axis=1, keepdims=True) + EPS)
        kb[unit] = kn.astype(BF16)
        kt[unit] = jnp.transpose(kn)
    for unit in units:
        turned = kt[unit].astype(BF16)
        grams[unit] = dot_nn(kb[unit], turned)
        mixes[unit] = dot_nn(read("q", *unit), turned)
    within, packed, corner, inverse = {}, {}, {}, {}
    for unit in units:
        head, span = unit
        cum, _, _, _, _, cols = spans[span]
        spread = cols[:, head : head + 1] - cum[head : head + 1, :]
        damp = jnp.where(lower, jnp.exp(jnp.minimum(spread, 0.0)), 0.0)
        within[unit] = (mixes[unit] * damp).astype(BF16)
        inner = jnp.where(strict, grams[unit] * damp * cols[:, heads + head : heads + head + 1], 0.0)
        pack = jnp.where(is_left, inner[:half], inner[half:])
        packed[unit] = pack.astype(BF16)
        corner[unit] = jnp.where(is_left, inner[half:], 0.0).astype(BF16)
        inverse[unit] = eye - pack * first
    for cut_left, cut_right in cuts:
        parts = {}
        for unit in units:
            piece = packed[unit]
            parts[unit] = dot_nn(
                inverse[unit].astype(BF16),
                jnp.concatenate([piece * cut_left, piece * cut_right], axis=0),
            )
        for unit in units:
            now = inverse[unit].astype(BF16)
            inverse[unit] = inverse[unit] - dot_nn(
                parts[unit].astype(BF16), jnp.concatenate([now * left, now * right], axis=0)
            )
    parts = {}
    for unit in units:
        now = inverse[unit].astype(BF16)
        parts[unit] = dot_nn(corner[unit], jnp.concatenate([now * left, now * right], axis=0))
    zeros = jnp.zeros((half, SPAN), BF16)
    full = {}
    for unit in units:
        now = inverse[unit]
        link = dot_nn(
            now.astype(BF16) * right, jnp.concatenate([zeros, parts[unit].astype(BF16)], axis=0)
        )
        full[unit] = jnp.concatenate(
            [jnp.where(is_left, now, 0.0), jnp.where(is_left, -link, now)], axis=0
        )
    base, key_mix, tails = {}, {}, {}
    for unit in units:
        head, span = unit
        _, beta, beta_grow, tail, _, _ = spans[span]
        base[unit] = dot_nn((full[unit] * beta[head : head + 1, :]).astype(BF16), read("v", *unit))
        key_mix[unit] = dot_nn(
            (full[unit] * beta_grow[head : head + 1, :]).astype(BF16), kb[unit]
        ).astype(BF16)
        tails[unit] = (kt[unit] * tail[head : head + 1, :]).astype(BF16)
    state = [jnp.zeros((head_dim, head_dim), F32) for _ in range(heads)]
    for span in range(count):
        reads = [
            dot_nn(
                jnp.concatenate([key_mix[head, span], read("q", head, span)], axis=0),
                state[head].astype(BF16),
            )
            for head in range(heads)
        ]
        fresh = [(base[head, span] - reads[head][:SPAN]).astype(BF16) for head in range(heads)]
        carry = spans[span][4]
        state = [
            state[head] * carry[head : head + 1, :] + dot_nn(tails[head, span], fresh[head])
            for head in range(heads)
        ]
        for head in range(heads):
            cols = spans[span][5]
            grow = cols[:, 2 * heads + head : 2 * heads + head + 1]
            result = reads[head][SPAN:] * grow + dot_nn(within[head, span], fresh[head])
            q32 = read("q", head, span).astype(F32)
            square = jnp.sum(q32 * q32, axis=1, keepdims=True)
            norm = lax.rsqrt(
                jnp.mean(result * result, axis=1, keepdims=True)
                + EPS * head_dim * (square + EPS)
            )
            store(head, span, result * norm * gain)


def whole_kernel(
    chips,
    head_dim,
    passage_rows,
    owners_ref,
    entries_ref,
    extra_ref,
    small_refs,
    gain_ref,
    rate_ref,
    tokens_hbm,
    store_hbm,
    weights_hbm,
    o_ref,
    tok,
    sto,
    wts,
    rq,
    qkv,
    kv_own,
    kv_sib,
    kv_out,
    qbuf,
    obuf,
    sbuf,
    part,
    pstat,
    normed,
    want_mine,
    want_all,
    want_smem,
    load_sem,
    want_sem,
    kv_sem,
    send_q,
    recv_q,
    send_r,
    recv_r,
    send_s,
    recv_s,
    send_w,
    recv_w,
):
    devices = 2 * chips
    reach = chips // 2
    me = lax.axis_index("st")
    core, chip = lax.rem(me, 2), me // 2
    other = 1 - core
    sibling = chip * 2 + other
    length, width = normed.shape
    half = width // 2
    heads = width // head_dim

    def device(dz, which):
        return lax.rem(chip + dz, chips) * 2 + which

    def rcopy(src, dst, ssem, rsem, target):
        return pltpu.make_async_remote_copy(
            src_ref=src,
            dst_ref=dst,
            send_sem=ssem,
            recv_sem=rsem,
            device_id={"st": target},
            device_id_type=pl.DeviceIdType.MESH,
        )

    barrier = pltpu.get_barrier_semaphore()

    @pl.loop(1, devices)
    def _(off):
        pl.semaphore_signal(
            barrier,
            inc=1,
            device_id={"st": lax.rem(me + off, devices)},
            device_id_type=pl.DeviceIdType.MESH,
        )

    rq_w, pk_w, pv_w, q_w = 0, 1, 2, 3
    loads = [pltpu.make_async_copy(tokens_hbm, tok, load_sem.at[0])]
    loads += [
        pltpu.make_async_copy(weights_hbm[i], wts.at[i], load_sem.at[1 + i]) for i in range(6)
    ]
    loads.append(pltpu.make_async_copy(store_hbm, sto, load_sem.at[7]))
    loads[0].start()
    loads[1].start()

    want_mine[...] = jnp.zeros_like(want_mine)
    per = owners_ref.shape[0]
    blocks = owners_ref.shape[1]
    want_mine[:per, :blocks] = owners_ref[...]
    want_mine[per : 2 * per, :blocks] = entries_ref[...]
    want_all[me] = want_mine[...]

    loads[0].wait()
    loads[1].wait()
    loads[7].start()
    loads[1 + pk_w].start()
    loads[1 + pv_w].start()

    @pl.loop(0, 2)
    def _(side):
        cols = pl.ds(pl.multiple_of(side * half, half), half)
        rq[side] = dot_nn(tok[...], wts[rq_w, :, cols]).astype(BF16)

    pl.semaphore_wait(barrier, devices - 1)

    def slot(dz, which):
        return (dz % chips) * 2 + which

    hop1 = []
    for count, (dz, which) in enumerate(
        [(1, core), (chips - 1, other), (1, other), (chips - 1, core)]
    ):
        there = slot(chips - dz, core)
        hop1.append(
            rcopy(
                rq.at[which], qbuf.at[there], send_q.at[count], recv_q.at[there], device(dz, which)
            )
        )
    hop1.append(
        rcopy(rq.at[other], qbuf.at[core], send_q.at[4], recv_q.at[core], sibling)
    )
    for copy in hop1:
        copy.start()

    def want_copy(off):
        return rcopy(
            want_mine,
            want_all.at[me],
            send_w.at[off - 1],
            recv_w.at[me],
            lax.rem(me + off, devices),
        )

    @pl.loop(1, devices)
    def _(off):
        want_copy(off).start()

    qbuf[core] = rq[core]

    loads[7].wait()
    loads[1 + pk_w].wait()
    for i in range(3):
        loads[1 + q_w + i].start()

    rows = sto.shape[0]
    tile = min(512, rows)

    def project_store(which, weight, dst, place):
        cols = pl.ds(pl.multiple_of(which * half, half), half)

        @pl.loop(0, rows // tile)
        def _(m):
            at = pl.ds(pl.multiple_of(m * tile, tile), tile)
            held = dot_nn(sto[at, :], wts[weight, :, cols]).astype(BF16)
            count = tile // passage_rows
            dst[pl.ds(m * count, count), :, place * half : (place + 1) * half] = held.reshape(
                count, passage_rows, half
            )

    project_store(other, pk_w, kv_out, 0)
    loads[1 + pv_w].wait()
    project_store(other, pv_w, kv_out, 1)
    project_store(core, pk_w, kv_own, 0)
    swap = rcopy(kv_out, kv_sib, kv_sem.at[0], kv_sem.at[1], sibling)
    swap.start()
    project_store(core, pv_w, kv_own, 1)

    for i in range(3):
        loads[1 + q_w + i].wait()

    @pl.loop(0, 6)
    def _(step):
        i, side = step // 2, lax.rem(step, 2)
        cols = pl.ds(pl.multiple_of(side * half, half), half)
        qkv[i, :, cols] = dot_nn(tok[...], wts[q_w + i, :, cols]).astype(BF16)

    small = jnp.concatenate(
        [ref[...] for ref in small_refs] + [jnp.zeros((16 - 3 * heads, tok.shape[1]), BF16)], axis=0
    )
    gates = dot_nt(tok[...], small)
    spans = gate_rows(gates, extra_ref, rate_ref)

    @pl.loop(1, devices)
    def _(off):
        source = lax.rem(me + off, devices)
        rcopy(want_mine, want_all.at[source], send_w.at[0], recv_w.at[source], source).wait_recv()

    fetch = pltpu.make_async_copy(want_all, want_smem, want_sem)
    fetch.start()
    fetch.wait()
    swap.wait()

    def await_query(at):
        rcopy(rq.at[0], qbuf.at[at], send_q.at[0], recv_q.at[at], sibling).wait_recv()

    def attend(dz, which):
        at = slot(dz, which)
        source = device(dz, which)

        def named(block):
            return [
                (want_smem[source, place, block], want_smem[source, per + place, block])
                for place in range(per)
            ]

        attend_unit(
            qbuf.at[at],
            named,
            me,
            sibling,
            kv_own,
            kv_sib,
            obuf.at[at],
            sbuf.at[at],
            passage_rows,
            head_dim,
        )

    def reply(dz, which):
        at = slot(dz, which)
        back = (chips - dz) % chips
        target = device(dz, which)
        return (
            rcopy(
                obuf.at[at], part.at[back, core], send_r.at[at], recv_r.at[back, core], target
            ),
            rcopy(
                sbuf.at[at], pstat.at[back, core], send_s.at[at], recv_s.at[back, core], target
            ),
        )

    relays = []

    def relay(src, dst, count, target):
        copy = rcopy(qbuf.at[src], qbuf.at[dst], send_q.at[count], recv_q.at[dst], target)
        copy.start()
        relays.append(copy)

    count = 5
    await_query(other)

    @pl.loop(0, 2)
    def _(which):
        attend(0, which)

    part[0, core] = obuf[core]
    pstat[0, core] = sbuf[core]
    for copy in reply(0, other):
        copy.start()

    for hop in range(1, reach):
        back = chips - hop
        if hop < reach - 1:
            for which in range(2):
                await_query(slot(back, which))
                relay(slot(back, which), slot(back - 1, which), count, device(1, core))
                await_query(slot(hop, which))
                relay(slot(hop, which), slot(hop + 1, which), count + 1, device(chips - 1, core))
                count += 2
        else:
            await_query(slot(back, core))
            relay(slot(back, core), slot(reach, core), count, device(1, core))
            await_query(slot(hop, other))
            relay(slot(hop, other), slot(reach, other), count + 1, device(chips - 1, core))
            count += 2
            await_query(slot(back, other))
            await_query(slot(hop, core))
        for dz in (back, hop):

            @pl.loop(0, 2)
            def _(which):
                attend(dz, which)
                for copy in reply(dz, which):
                    copy.start()

    await_query(slot(reach, 0))
    await_query(slot(reach, 1))

    @pl.loop(0, 2)
    def _(which):
        attend(reach, which)
        for copy in reply(reach, which):
            copy.start()

    def read(name, head, span):
        return qkv[
            "qkv".index(name),
            span * SPAN : (span + 1) * SPAN,
            head * head_dim : (head + 1) * head_dim,
        ]

    def keep(head, span, value):
        normed[span * SPAN : (span + 1) * SPAN, head * head_dim : (head + 1) * head_dim] = value

    delta_body(spans, read, gain_ref[...], heads, keep)

    def await_part(back, side):
        rcopy(
            obuf.at[0], part.at[back, side], send_r.at[0], recv_r.at[back, side], sibling
        ).wait_recv()
        rcopy(
            sbuf.at[0], pstat.at[back, side], send_s.at[0], recv_s.at[back, side], sibling
        ).wait_recv()

    await_part(0, other)
    for back in range(1, chips):
        for side in range(2):
            await_part(back, side)

    here = heads // 2
    for side in range(2):
        stats = [pstat[back, side] for back in range(chips)]
        peak = functools.reduce(jnp.maximum, stats)
        expo = [jnp.exp(stat - peak) for stat in stats]
        inv = 1.0 / functools.reduce(jnp.add, expo)
        shares = [jnp.transpose(e * inv) for e in expo]
        for block in range(blocks):
            at = slice(block * BLOCK, (block + 1) * BLOCK)
            span, inside = divmod(block * BLOCK, SPAN)
            for local in range(here):
                cols = slice(local * head_dim, (local + 1) * head_dim)
                head = side * here + local
                where = slice(head * head_dim, (head + 1) * head_dim)
                value = functools.reduce(
                    jnp.add,
                    [
                        part[back, side, at, cols].astype(F32)
                        * shares[back][local * BLOCK : (local + 1) * BLOCK, block : block + 1]
                        for back in range(chips)
                    ],
                )
                rgate = spans[span][5][
                    inside : inside + BLOCK, 3 * heads + head : 3 * heads + head + 1
                ]
                o_ref[at, where] = (normed[at, where] + rgate * value).astype(BF16)

    for copy in hop1 + relays:
        copy.wait_send()

    @pl.loop(1, devices)
    def _(off):
        want_copy(off).wait_send()

    for copy in reply(0, other):
        copy.wait_send()
    for dz in range(1, chips):
        for which in range(2):
            for copy in reply(dz, which):
                copy.wait_send()


def per_device(
    chips,
    tokens,
    owners,
    entries,
    store,
    mixer_query_weight,
    mixer_key_weight,
    mixer_value_weight,
    strength_weight,
    decay_weight,
    head_decay_rate,
    extra_forgetting_exponent,
    output_norm_gain,
    retrieval_query_weight,
    passage_key_weight,
    passage_value_weight,
    retrieval_gate_weight,
):
    heads = head_decay_rate.shape[0]
    head_dim = output_norm_gain.shape[0]
    length, depth = tokens.shape
    passage_rows = store.shape[1]
    rows = store.shape[0] * passage_rows
    width = heads * head_dim
    half = width // 2
    devices = 2 * chips
    blocks = owners.shape[0]
    vmem = pl.BlockSpec(memory_space=pltpu.VMEM)
    anywhere = pl.BlockSpec(memory_space=pl.ANY)
    weights = [
        retrieval_query_weight,
        passage_key_weight,
        passage_value_weight,
        mixer_query_weight,
        mixer_key_weight,
        mixer_value_weight,
    ]

    def body(owners_ref, entries_ref, extra_ref, s1, s2, s3, gain_ref, rate_ref, tok, sto, *rest):
        whole_kernel(
            chips, head_dim, passage_rows, owners_ref, entries_ref, extra_ref, (s1, s2, s3),
            gain_ref, rate_ref, tok, sto, rest[:6], *rest[6:],
        )

    dma = pltpu.SemaphoreType.DMA
    return pl.pallas_call(
        body,
        out_shape=jax.ShapeDtypeStruct((length, width), BF16),
        in_specs=[vmem] * 7 + [pl.BlockSpec(memory_space=pltpu.SMEM)] + [anywhere] * 8,
        out_specs=vmem,
        scratch_shapes=[
            pltpu.VMEM((length, depth), BF16),
            pltpu.VMEM((rows, depth), BF16),
            pltpu.VMEM((6, depth, width), BF16),
            pltpu.VMEM((2, length, half), BF16),
            pltpu.VMEM((3, length, width), BF16),
            pltpu.VMEM((store.shape[0], passage_rows, width), BF16),
            pltpu.VMEM((store.shape[0], passage_rows, width), BF16),
            pltpu.VMEM((store.shape[0], passage_rows, width), BF16),
            pltpu.VMEM((devices, length, half), BF16),
            pltpu.VMEM((devices, length, half), BF16),
            pltpu.VMEM((devices, blocks, 2 * BLOCK), F32),
            pltpu.VMEM((chips, 2, length, half), BF16),
            pltpu.VMEM((chips, 2, blocks, 2 * BLOCK), F32),
            pltpu.VMEM((length, width), F32),
            pltpu.VMEM((8, 128), jnp.int32),
            pltpu.VMEM((devices, 8, 128), jnp.int32),
            pltpu.SMEM((devices, 8, 128), jnp.int32),
            dma((8,)),
            dma,
            dma((2,)),
            dma((5 + 2 * devices,)),
            dma((devices,)),
            dma((devices,)),
            dma((chips, 2)),
            dma((devices,)),
            dma((chips, 2)),
            dma((devices,)),
            dma((devices,)),
        ],
        compiler_params=pltpu.CompilerParams(
            collective_id=0, has_side_effects=True, vmem_limit_bytes=60 * 1024 * 1024
        ),
        cost_estimate=pl.CostEstimate(
            flops=12_000_000_000, bytes_accessed=20_000_000, transcendentals=0
        ),
        name="whole",
    )(
        owners.T,
        entries.T,
        extra_forgetting_exponent.T,
        strength_weight.T,
        decay_weight.T,
        retrieval_gate_weight.T,
        output_norm_gain[None, :],
        head_decay_rate,
        tokens,
        store.reshape(rows, depth),
        *weights,
    )


def solution(mesh):
    rows = ("grp", "st")
    return jax.shard_map(
        functools.partial(per_device, mesh.shape["st"] // 2),
        mesh=mesh,
        in_specs=(
            P(rows, None),
            P(rows, None),
            P(rows, None),
            P(rows, None, None),
            P(None, "tp"),
            P(None, "tp"),
            P(None, "tp"),
            P(None, "tp"),
            P(None, "tp"),
            P("tp"),
            P(rows, "tp"),
            P(),
            P(None, "tp"),
            P(None, "tp"),
            P(None, "tp"),
            P(None, "tp"),
        ),
        out_specs=P(rows, "tp"),
        check_vma=False,
    )
```

profile of v0, /device:TPU:1, one launch (start us, length us, event | category | flops | bytes accessed | tf_op | source)
XLA Modules:
  0.0 98.6 jit_solution(6784568384407507790)
XLA Ops:
  0.0 96.8 %whole.1 = bf16[512,512]{1,0:T(8,128)(2,1)} custom-call(s32[4,8]{1,0:T(4,128)} %bitcast.13, s32[4,8]{1,0:T(4,128)} %bitcast.14, f32[4,512]{1,0:T(4,128)} %bitcast.12, bf16[4,2048]{1,0:T(4,128)(2,1)} %bitcast.9, bf16[4,2048]{1,0:T(4,128)(2,1)} %bitcast.10, bf16[4,2048]{1,0:T(4,128)(2,1)} %bitcast.11, f32[1,128]{1,0:T(1,128)} %bitcast.15, f32[4]{0:T(128)} %rate_ref.1, ...), custom_call_target="tpu_custom_call" | custom-call | flops 12000000000 | bytes 20000000 | tf_op jit(solution)/shard_map/whole/pallas_call | solution.py:656
  96.8 1.9 %copy.18 = bf16[512,512]{1,0:T(8,128)(2,1)} copy(bf16[512,512]{1,0:T(8,128)(2,1)} %whole.1) | data formatting | bytes 1048576
where the time goes:
time: 98.8 us; the launch traced here: 98.6 us
  Pallas kernels  96.8 us (98%)
  local copies, waits for them, and re-layouts  1.87 us (2%)
    pallas_call x1, Pallas kernels, per_device(): pl.pallas_call(body, out_shape=jax.ShapeDtypeStruct((length, width), BF16...  96.8 us

commit v1 on v0

--- a/solution.py
+++ b/solution.py
@@ -27,10 +27,9 @@
     return lax.dot_general(left, right, (((0,), (0,)), ((), ())), preferred_element_type=F32)
 
 
-def attend_unit(q_ref, named, me, sibling, kv_own, kv_sib, o_ref, stat_ref, passage_rows, head_dim):
-    length, half = q_ref.shape
+def attend_jobs(jobs, me, sibling, kv_own, kv_sib, head_dim):
+    passage_rows, half = kv_own.shape[1], kv_own.shape[2] // 2
     heads = half // head_dim
-    blocks = length // BLOCK
     scale = head_dim ** (-0.5)
     nothing = jnp.zeros((BLOCK, head_dim), BF16)
 
@@ -41,12 +40,13 @@
         found = jnp.minimum(hit, 1)
         return hit - found, (1 - found).astype(F32) * MISSING
 
-    places, scores = [], []
-    for block in range(blocks):
-        pairs = named(block)
-        row_own, bias_own = find(pairs, me)
-        row_sib, bias_sib = find(pairs, sibling)
-        places.append((row_own, bias_own, row_sib, bias_sib))
+    work = []
+    for q_ref, named, o_ref, stat_ref in jobs:
+        for block in range(q_ref.shape[0] // BLOCK):
+            pairs = named(block)
+            work.append((q_ref, o_ref, block, find(pairs, me), find(pairs, sibling)))
+    scores = []
+    for q_ref, _, block, (row_own, _), (row_sib, _) in work:
         query = q_ref[block * BLOCK : (block + 1) * BLOCK, :]
         spread = jnp.concatenate(
             [
@@ -61,18 +61,10 @@
             ],
             axis=0,
         )
-        keys = jnp.concatenate(
-            [
-                kv_own[row_own, :, :half],
-                kv_sib[row_sib, :, :half],
-            ],
-            axis=0,
-        )
+        keys = jnp.concatenate([kv_own[row_own, :, :half], kv_sib[row_sib, :, :half]], axis=0)
         scores.append(dot_nt(keys, spread))
     weights, stats = [], []
-    for block in range(blocks):
-        _, bias_own, _, bias_sib = places[block]
-        raw = scores[block]
+    for (_, _, _, (_, bias_own), (_, bias_sib)), raw in zip(work, scores):
         own = raw[:passage_rows] * scale + bias_own
         sib = raw[passage_rows:] * scale + bias_sib
         peak = jnp.max(jnp.maximum(own, sib), axis=0, keepdims=True)
@@ -82,26 +74,47 @@
         inv = 1.0 / total
         weights.append(jnp.concatenate([e_own * inv, e_sib * inv], axis=0).astype(BF16))
         stats.append(peak + jnp.log(total))
-    for block in range(blocks):
-        row_own, _, row_sib, _ = places[block]
-        values = jnp.concatenate(
-            [
-                kv_own[row_own, :, half:],
-                kv_sib[row_sib, :, half:],
-            ],
-            axis=0,
-        )
-        result = dot_tn(weights[block], values)
+    for (_, o_ref, block, (row_own, _), (row_sib, _)), weight in zip(work, weights):
+        values = jnp.concatenate([kv_own[row_own, :, half:], kv_sib[row_sib, :, half:]], axis=0)
+        result = dot_tn(weight, values)
         for head in range(heads):
             cols = slice(head * head_dim, (head + 1) * head_dim)
             o_ref[block * BLOCK : (block + 1) * BLOCK, cols] = result[
                 head * BLOCK : (head + 1) * BLOCK, cols
             ].astype(BF16)
-    rows = jnp.concatenate(stats, axis=0)
-    spare = stat_ref.shape[1] - rows.shape[1]
-    if spare:
-        rows = jnp.concatenate([rows, jnp.zeros((blocks, spare), F32)], axis=1)
-    stat_ref[...] = rows
+    done = 0
+    for q_ref, _, _, stat_ref in jobs:
+        blocks = q_ref.shape[0] // BLOCK
+        rows = jnp.concatenate(stats[done : done + blocks], axis=0)
+        done += blocks
+        spare = stat_ref.shape[1] - rows.shape[1]
+        if spare:
+            rows = jnp.concatenate([rows, jnp.zeros((blocks, spare), F32)], axis=1)
+        stat_ref[...] = rows
+
+
+def shares_of(stats):
+    peak = functools.reduce(jnp.maximum, stats)
+    expo = [jnp.exp(stat - peak) for stat in stats]
+    total = functools.reduce(jnp.add, expo)
+    inv = 1.0 / total
+    pad = (-peak.shape[0]) % 8
+    rows = [e * inv for e in expo]
+    if pad:
+        rows = [jnp.concatenate([r, jnp.zeros((pad, r.shape[1]), F32)], axis=0) for r in rows]
+    return [jnp.transpose(r) for r in rows], peak + jnp.log(total)
+
+
+def blend(refs, shares, block, local, head_dim):
+    at = slice(block * BLOCK, (block + 1) * BLOCK)
+    cols = slice(local * head_dim, (local + 1) * head_dim)
+    return functools.reduce(
+        jnp.add,
+        [
+            ref[at, cols].astype(F32) * share[local * BLOCK : (local + 1) * BLOCK, block : block + 1]
+            for ref, share in zip(refs, shares)
+        ],
+    )
 
 
 def gate_rows(gates, extra_ref, rate_ref):
@@ -135,7 +148,7 @@
         ends = cum[:, SPAN - 1 : SPAN]
         grow = jnp.exp(cum)
         cols = jnp.transpose(jnp.concatenate([cum, beta[:, at], grow, rgate[:, at]], axis=0))
-        spans.append((cum, beta[:, at], beta[:, at] * grow, jnp.exp(ends - cum), jnp.exp(ends), cols))
+        spans.append((cum, beta[:, at], beta[:, at] * grow, jnp.exp(ends - cum), jnp.exp(ends), cols, rgate[:, at]))
     return spans
 
 
@@ -182,7 +195,7 @@
     within, packed, corner, inverse = {}, {}, {}, {}
     for unit in units:
         head, span = unit
-        cum, _, _, _, _, cols = spans[span]
+        cum, _, _, _, _, cols, _ = spans[span]
         spread = cols[:, head : head + 1] - cum[head : head + 1, :]
         damp = jnp.where(lower, jnp.exp(jnp.minimum(spread, 0.0)), 0.0)
         within[unit] = (mixes[unit] * damp).astype(BF16)
@@ -221,7 +234,7 @@
     base, key_mix, tails = {}, {}, {}
     for unit in units:
         head, span = unit
-        _, beta, beta_grow, tail, _, _ = spans[span]
+        _, beta, beta_grow, tail, _, _, _ = spans[span]
         base[unit] = dot_nn((full[unit] * beta[head : head + 1, :]).astype(BF16), read("v", *unit))
         key_mix[unit] = dot_nn(
             (full[unit] * beta_grow[head : head + 1, :]).astype(BF16), kb[unit]
@@ -256,6 +269,808 @@
 
 
 def whole_kernel(
+    chips,
+    head_dim,
+    passage_rows,
+    lesser,
+    tokens_hbm,
+    store_hbm,
+    weights_hbm,
+    o_ref,
+    owners_ref,
+    entries_ref,
+    extra_ref,
+    small_a,
+    small_b,
+    small_c,
+    gain_ref,
+    rate_ref,
+    gate_ref,
+    tok,
+    sto,
+    wts,
+    rq,
+    qkv,
+    kv_own,
+    kv_sib,
+    kv_out,
+    qbuf,
+    obuf,
+    sbuf,
+    rbuf,
+    rstat,
+    fin,
+    fstat,
+    normed,
+    gsel,
+    want_mine,
+    want_all,
+    want_smem,
+    load_sem,
+    want_sem,
+    kv_sem,
+    send_q,
+    recv_q,
+    send_r,
+    send_s,
+    recv_r,
+    recv_s,
+    recv_f,
+    recv_g,
+    send_w,
+    recv_w,
+    send_h,
+):
+    devices = 2 * chips
+    reach = chips // 2
+    me = lax.axis_index("st")
+    core, chip = lax.rem(me, 2), me // 2
+    other = 1 - core
+    sibling = chip * 2 + other
+    length, width = normed.shape
+    half = width // 2
+    heads = width // head_dim
+    here = heads // 2
+    pieces = rq.shape[1]
+    piece_rows = length // pieces
+    piece_blocks = piece_rows // BLOCK
+    per = owners_ref.shape[0]
+    blocks = owners_ref.shape[1]
+
+    def rcopy(src, dst, ssem, rsem, target):
+        return pltpu.make_async_remote_copy(
+            src_ref=src,
+            dst_ref=dst,
+            send_sem=ssem,
+            recv_sem=rsem,
+            device_id={"st": target},
+            device_id_type=pl.DeviceIdType.MESH,
+        )
+
+    barrier = pltpu.get_barrier_semaphore()
+
+    @pl.loop(1, devices)
+    def _(off):
+        pl.semaphore_signal(
+            barrier,
+            inc=1,
+            device_id={"st": lax.rem(me + off, devices)},
+            device_id_type=pl.DeviceIdType.MESH,
+        )
+
+    rq_w, pk_w, pv_w, q_w = 0, 1, 2, 3
+
+    def token_rows(piece):
+        at = pl.ds(piece * piece_rows, piece_rows)
+        return pltpu.make_async_copy(tokens_hbm.at[at], tok.at[at], load_sem.at[8 + piece])
+
+    def query_weight(which, index):
+        at = pl.ds(pl.multiple_of(which * half, half), half)
+        return pltpu.make_async_copy(
+            weights_hbm[rq_w].at[:, at], wts.at[rq_w, :, at], load_sem.at[index]
+        )
+
+    loads = [None, None]
+    loads += [
+        pltpu.make_async_copy(weights_hbm[i], wts.at[i], load_sem.at[1 + i]) for i in range(1, 6)
+    ]
+    loads.append(pltpu.make_async_copy(store_hbm, sto, load_sem.at[7]))
+    first_loads = [token_rows(0), query_weight(core, 0)]
+    second_loads = [token_rows(piece) for piece in range(1, pieces)] + [query_weight(other, 1)]
+    small_refs = (small_a, small_b, small_c)
+    lesser_loads = [
+        pltpu.make_async_copy(src, dst, load_sem.at[8 + pieces + i])
+        for i, (src, dst) in enumerate(
+            zip(lesser, (owners_ref, entries_ref, extra_ref) + small_refs + (gain_ref, rate_ref))
+        )
+    ]
+    for copy in first_loads + lesser_loads[:2] + second_loads:
+        copy.start()
+    lesser_loads[0].wait()
+    lesser_loads[1].wait()
+
+    want_mine[...] = jnp.zeros_like(want_mine)
+    want_mine[:per, :blocks] = owners_ref[...]
+    want_mine[per : 2 * per, :blocks] = entries_ref[...]
+    want_all[me] = want_mine[...]
+
+    with jax.named_scope("wait_tok"):
+        for copy in first_loads:
+            copy.wait()
+    loads[7].start()
+    loads[1 + pk_w].start()
+
+    def project_query(side, piece):
+        at = pl.ds(piece * piece_rows, piece_rows)
+        cols = pl.ds(pl.multiple_of(side * half, half), half)
+        rq[side, piece] = dot_nn(tok[at, :], wts[rq_w, :, cols]).astype(BF16)
+
+    def want_copy(off):
+        return rcopy(
+            want_mine,
+            want_all.at[me],
+            send_w.at[off - 1],
+            recv_w.at[me],
+            lax.rem(me + off, devices),
+        )
+
+    def own_query(there, side, piece, way):
+        return rcopy(
+            rq.at[side, piece],
+            qbuf.at[me, piece],
+            send_q.at[way, chip * 2 + side, piece],
+            recv_q.at[me, piece],
+            there * 2 + side,
+        )
+
+    def pass_query(source, piece, there, way):
+        return rcopy(
+            qbuf.at[source, piece],
+            qbuf.at[source, piece],
+            send_q.at[way, source, piece],
+            recv_q.at[source, piece],
+            there * 2 + core,
+        )
+
+    def await_query(source, piece):
+        pass_query(source, piece, sibling // 2, 0).wait_recv()
+
+    def result_to(source, piece, dst, dstat, rsem, gsem, target):
+        return (
+            rcopy(obuf.at[source, piece], dst, send_r.at[source, piece], rsem, target),
+            rcopy(sbuf.at[source, piece], dstat, send_s.at[source, piece], gsem, target),
+        )
+
+    def pass_result(source, piece, there):
+        return result_to(
+            source,
+            piece,
+            rbuf.at[source, piece],
+            rstat.at[source, piece],
+            recv_r.at[source, piece],
+            recv_s.at[source, piece],
+            there * 2 + core,
+        )
+
+    def give_result(source, piece, side):
+        return result_to(
+            source,
+            piece,
+            fin.at[side, core, piece],
+            fstat.at[side, core, piece],
+            recv_f.at[side, core, piece],
+            recv_g.at[side, core, piece],
+            source,
+        )
+
+    def await_result(source, piece):
+        for copy in pass_result(source, piece, sibling // 2):
+            copy.wait_recv()
+
+    def await_final(side, which, piece):
+        copies = result_to(
+            me,
+            piece,
+            fin.at[side, which, piece],
+            fstat.at[side, which, piece],
+            recv_f.at[side, which, piece],
+            recv_g.at[side, which, piece],
+            sibling,
+        )
+        for copy in copies:
+            copy.wait_recv()
+
+    def begin(copies):
+        for copy in copies if isinstance(copies, tuple) else (copies,):
+            copy.start()
+
+    def job(source, piece, own=False):
+        def named(block):
+            at = piece * piece_blocks + block
+            return [
+                (want_smem[source, place, at], want_smem[source, per + place, at])
+                for place in range(per)
+            ]
+
+        if own:
+            return (
+                rq.at[core, piece], named, fin.at[2, core, piece], fstat.at[2, core, piece]
+            )
+        return (qbuf.at[source, piece], named, obuf.at[source, piece], sbuf.at[source, piece])
+
+    def attend(*jobs):
+        attend_jobs(jobs, me, sibling, kv_own, kv_sib, head_dim)
+
+    def attend_here():
+        @pl.loop(0, pieces)
+        def _(piece):
+            await_query(sibling, piece)
+            attend(job(me, piece, own=True), job(sibling, piece))
+            begin(give_result(sibling, piece, 2))
+
+    def merge(source, piece):
+        await_result(source, piece)
+        refs = [obuf.at[source, piece], rbuf.at[source, piece]]
+        shares, stat = shares_of([sbuf[source, piece], rstat[source, piece]])
+        for block in range(piece_blocks):
+            for local in range(here):
+                value = blend(refs, shares, block, local, head_dim)
+                obuf[
+                    source,
+                    piece,
+                    block * BLOCK : (block + 1) * BLOCK,
+                    local * head_dim : (local + 1) * head_dim,
+                ] = value.astype(BF16)
+        sbuf[source, piece] = stat
+
+    inner = jnp.logical_and(chip > 0, chip < chips - 1)
+    end = jnp.logical_or(chip == 0, chip == chips - 1)
+    near = 2 * (chip // reach) - 1
+    far = -near
+    near_side, far_side = (1 - near) // 2, (1 - far) // 2
+
+    def own_first(piece):
+        @pl.when(inner)
+        def _():
+            own_query(chip + near, core, piece, 0).start()
+            own_query(chip + far, core, piece, 1).start()
+
+        @pl.when(end)
+        def _():
+            own_query(chip + far, core, piece, 1).start()
+
+    with jax.named_scope("rq0"):
+        project_query(core, 0)
+    with jax.named_scope("barrier_wait"):
+        pl.semaphore_wait(barrier, devices - 1)
+    with jax.named_scope("rq1"):
+
+        @pl.loop(1, devices)
+        def _(off):
+            want_copy(off).start()
+
+        own_first(0)
+        for copy in second_loads:
+            copy.wait()
+        for copy in lesser_loads[2:]:
+            copy.start()
+        loads[1 + pv_w].start()
+        for piece in range(1, pieces):
+            project_query(core, piece)
+            own_first(piece)
+        for piece in range(pieces):
+            project_query(other, piece)
+
+    @pl.when(end)
+    def _():
+        for piece in range(pieces):
+            own_query(chip + far, other, piece, 1).start()
+
+    def sib_copy(piece):
+        return rcopy(
+            rq.at[other, piece], qbuf.at[me, piece], send_h.at[piece], recv_q.at[me, piece], sibling
+        )
+
+    rows = sto.shape[0]
+    tile = min(512, rows)
+
+    def project_store(which, weight, dst, place, m):
+        cols = pl.ds(pl.multiple_of(which * half, half), half)
+        at = pl.ds(pl.multiple_of(m * tile, tile), tile)
+        held = dot_nn(sto[at, :], wts[weight, :, cols]).astype(BF16)
+        count = tile // passage_rows
+        dst[pl.ds(m * count, count), :, place * half : (place + 1) * half] = held.reshape(
+            count, passage_rows, half
+        )
+
+    def relay_first(piece):
+        edge, peer = chip + near, chip + far
+
+        @pl.when(inner)
+        def _():
+            await_query(edge * 2 + core, piece)
+            pass_query(edge * 2 + core, piece, peer, 1).start()
+            await_query(peer * 2 + core, piece)
+            pass_query(peer * 2 + core, piece, edge, 0).start()
+
+    tiles = rows // tile
+    with jax.named_scope("kv"):
+        loads[7].wait()
+        loads[1 + pk_w].wait()
+        for i in range(3):
+            loads[1 + q_w + i].start()
+
+        @pl.loop(0, tiles)
+        def _(m):
+            project_store(other, pk_w, kv_out, 0, m)
+
+        loads[1 + pv_w].wait()
+
+        @pl.loop(0, tiles)
+        def _(m):
+            project_store(other, pv_w, kv_out, 1, m)
+
+        swap = rcopy(kv_out, kv_sib, kv_sem.at[0], kv_sem.at[1], sibling)
+        swap.start()
+        for piece in range(pieces):
+            sib_copy(piece).start()
+
+        @pl.loop(0, tiles)
+        def _(m):
+            project_store(core, pk_w, kv_own, 0, m)
+
+    with jax.named_scope("relay0"):
+        relay_first(0)
+    with jax.named_scope("kv2"):
+
+        @pl.loop(0, tiles)
+        def _(m):
+            project_store(core, pv_w, kv_own, 1, m)
+
+    with jax.named_scope("relay1"):
+        for piece in range(1, pieces):
+            relay_first(piece)
+
+    def project_mixer(step):
+        i, side = step // 2, lax.rem(step, 2)
+        cols = pl.ds(pl.multiple_of(side * half, half), half)
+        qkv[i, :, cols] = dot_nn(tok[...], wts[q_w + i, :, cols]).astype(BF16)
+
+    def project_gates():
+        small = jnp.concatenate(
+            [ref[...] for ref in small_refs]
+            + [jnp.zeros((16 - 3 * heads, tok.shape[1]), BF16)],
+            axis=0,
+        )
+        gate_ref[...] = dot_nt(tok[...], small)
+
+    with jax.named_scope("wants"):
+
+        @pl.loop(1, devices)
+        def _(off):
+            source = lax.rem(me + off, devices)
+            rcopy(want_mine, want_all.at[source], send_w.at[0], recv_w.at[source], source).wait_recv()
+
+        fetch = pltpu.make_async_copy(want_all, want_smem, want_sem)
+        fetch.start()
+        fetch.wait()
+        swap.wait()
+        for i in range(3):
+            loads[1 + q_w + i].wait()
+        for copy in lesser_loads[2:]:
+            copy.wait()
+
+    @pl.when(inner)
+    def _():
+        edge, peer, beyond = chip + near, chip + far, chip + 2 * far
+
+        def at(where, which):
+            return where * 2 + which
+
+        with jax.named_scope("in01"):
+
+            @pl.loop(0, pieces)
+            def _(piece):
+                attend(job(at(edge, core), piece), job(at(peer, core), piece))
+
+        with jax.named_scope("in_here"):
+            attend_here()
+        with jax.named_scope("in23"):
+
+            @pl.loop(0, pieces)
+            def _(piece):
+                await_query(at(edge, other), piece)
+                pass_query(at(edge, other), piece, peer, 1).start()
+                await_query(at(beyond, core), piece)
+                pass_query(at(beyond, core), piece, edge, 0).start()
+                attend(job(at(edge, other), piece), job(at(beyond, core), piece))
+
+                @pl.loop(2 * piece, 2 * piece + 2)
+                def _(step):
+                    project_mixer(step)
+
+
+        for piece in range(pieces):
+            own_query(peer, other, piece, 1).start()
+        with jax.named_scope("in45"):
+
+            @pl.loop(0, pieces)
+            def _(piece):
+                await_query(at(beyond, other), piece)
+                pass_query(at(beyond, other), piece, edge, 0).start()
+                attend(job(at(beyond, other), piece))
+                project_mixer(2 * pieces + piece)
+
+        project_gates()
+        with jax.named_scope("in67"):
+
+            @pl.loop(0, pieces)
+            def _(piece):
+                await_query(at(peer, other), piece)
+                pass_query(at(peer, other), piece, edge, 0).start()
+                merge(at(beyond, core), piece)
+                begin(pass_result(at(beyond, core), piece, peer))
+                attend(job(at(peer, other), piece))
+
+        for piece in range(pieces):
+            own_query(edge, other, piece, 0).start()
+        with jax.named_scope("in89"):
+
+            @pl.loop(0, pieces)
+            def _(piece):
+                merge(at(beyond, other), piece)
+                begin(pass_result(at(beyond, other), piece, peer))
+                merge(at(edge, core), piece)
+                begin(give_result(at(edge, core), piece, near_side))
+
+        with jax.named_scope("in1011"):
+
+            @pl.loop(0, pieces)
+            def _(piece):
+                merge(at(peer, core), piece)
+                begin(give_result(at(peer, core), piece, far_side))
+                merge(at(edge, other), piece)
+                begin(give_result(at(edge, other), piece, near_side))
+
+        with jax.named_scope("in12"):
+
+            @pl.loop(0, pieces)
+            def _(piece):
+                merge(at(peer, other), piece)
+                begin(give_result(at(peer, other), piece, far_side))
+
+    @pl.when(end)
+    def _():
+        def at(distance, which):
+            return (chip + far * distance) * 2 + which
+
+        def handle(distance, which, send, fill=None):
+            @pl.loop(0, pieces)
+            def _(piece):
+                await_query(at(distance, which), piece)
+                attend(job(at(distance, which), piece))
+                if send:
+                    if distance == 1:
+                        begin(give_result(at(distance, which), piece, far_side))
+                    else:
+                        begin(pass_result(at(distance, which), piece, chip + far))
+                if fill is not None:
+                    fill(piece)
+
+        def fill_two(piece):
+            @pl.loop(2 * piece, 2 * piece + 2)
+            def _(step):
+                project_mixer(step)
+
+        def fill_one(piece):
+            project_mixer(2 * pieces + piece)
+
+        with jax.named_scope("end01"):
+            handle(1, core, False)
+        with jax.named_scope("end_here"):
+            attend_here()
+        with jax.named_scope("end23"):
+            handle(2, core, True, fill_two)
+        with jax.named_scope("end45"):
+            handle(3, core, True, fill_one)
+        project_gates()
+        with jax.named_scope("end67"):
+            handle(3, other, True)
+        with jax.named_scope("end89"):
+            handle(2, other, True)
+        for piece in range(pieces):
+            begin(give_result(at(1, core), piece, far_side))
+        with jax.named_scope("end1011"):
+            handle(1, other, True)
+
+    with jax.named_scope("gates"):
+        spans = gate_rows(gate_ref[...], extra_ref, rate_ref)
+        for span, held in enumerate(spans):
+            for side in range(2):
+                rgate = held[6][side * here : (side + 1) * here]
+                gsel[side, span * SPAN : (span + 1) * SPAN, :8] = jnp.transpose(
+                    jnp.concatenate([rgate, jnp.zeros((8 - here, SPAN), F32)], axis=0)
+                )
+
+    def read(name, head, span):
+        return qkv[
+            "qkv".index(name),
+            span * SPAN : (span + 1) * SPAN,
+            head * head_dim : (head + 1) * head_dim,
+        ]
+
+    def keep(head, span, value):
+        normed[span * SPAN : (span + 1) * SPAN, head * head_dim : (head + 1) * head_dim] = value
+
+    with jax.named_scope("delta"):
+        delta_body(spans, read, gain_ref[...], heads, keep)
+
+    def finish(which, piece, sides):
+        @pl.when(which == other)
+        def _():
+            await_final(2, which, piece)
+
+        for side in sides[:-1]:
+            await_final(side, which, piece)
+        refs = [fin.at[side, which, piece] for side in sides]
+        shares, _ = shares_of([fstat[side, which, piece] for side in sides])
+        for block in range(piece_blocks):
+            at = pl.ds(pl.multiple_of(piece * piece_rows + block * BLOCK, BLOCK), BLOCK)
+            for local in range(here):
+                cols = pl.ds(
+                    pl.multiple_of(which * half + local * head_dim, head_dim), head_dim
+                )
+                value = blend(refs, shares, block, local, head_dim)
+                rgate = gsel[which, at, local : local + 1]
+                o_ref[at, cols] = (normed[at, cols] + rgate * value).astype(BF16)
+
+    def finish_all(sides):
+        @pl.loop(0, 2 * pieces)
+        def _(step):
+            finish(lax.rem(core + step // pieces, 2), lax.rem(step, pieces), sides)
+
+    with jax.named_scope("finish"):
+
+        @pl.when(inner)
+        def _():
+            finish_all((0, 1, 2))
+
+        @pl.when(end)
+        def _():
+            finish_all((1 - far_side, 2))
+
+    @pl.loop(1, devices)
+    def _(off):
+        want_copy(off).wait_send()
+
+    @pl.loop(0, pieces)
+    def _(piece):
+        sib_copy(piece).wait_send()
+        for copy in give_result(sibling, piece, 2):
+            copy.wait_send()
+
+    @pl.loop(0, 2 * pieces)
+    def _(step):
+        piece, which = lax.rem(step, pieces), step // pieces
+
+        @pl.when(inner)
+        def _():
+            edge, peer, beyond = chip + near, chip + far, chip + 2 * far
+            own_query(edge, which, piece, 0).wait_send()
+            own_query(peer, which, piece, 1).wait_send()
+            pass_query(edge * 2 + which, piece, peer, 1).wait_send()
+            pass_query(peer * 2 + which, piece, edge, 0).wait_send()
+            pass_query(beyond * 2 + which, piece, edge, 0).wait_send()
+            for where in (edge, peer, beyond):
+                for copy in give_result(where * 2 + which, piece, 0):
+                    copy.wait_send()
+
+        @pl.when(end)
+        def _():
+            own_query(chip + far, which, piece, 1).wait_send()
+            for distance in range(1, chips):
+                for copy in give_result((chip + far * distance) * 2 + which, piece, 0):
+                    copy.wait_send()
+
+
+def line_device(
+    chips,
+    tokens,
+    owners,
+    entries,
+    store,
+    mixer_query_weight,
+    mixer_key_weight,
+    mixer_value_weight,
+    strength_weight,
+    decay_weight,
+    head_decay_rate,
+    extra_forgetting_exponent,
+    output_norm_gain,
+    retrieval_query_weight,
+    passage_key_weight,
+    passage_value_weight,
+    retrieval_gate_weight,
+):
+    heads = head_decay_rate.shape[0]
+    head_dim = output_norm_gain.shape[0]
+    length, depth = tokens.shape
+    passage_rows = store.shape[1]
+    rows = store.shape[0] * passage_rows
+    width = heads * head_dim
+    half = width // 2
+    devices = 2 * chips
+    blocks = owners.shape[0]
+    pieces = 2
+    piece_rows, piece_blocks = length // pieces, blocks // pieces
+    lanes = 2 * BLOCK
+    vmem = pl.BlockSpec(memory_space=pltpu.VMEM)
+    anywhere = pl.BlockSpec(memory_space=pl.ANY)
+    weights = [
+        retrieval_query_weight,
+        passage_key_weight,
+        passage_value_weight,
+        mixer_query_weight,
+        mixer_key_weight,
+        mixer_value_weight,
+    ]
+
+    def body(*refs):
+        whole_kernel(
+            chips, head_dim, passage_rows, refs[:8], refs[8], refs[9], refs[10:16], *refs[16:]
+        )
+
+    dma = pltpu.SemaphoreType.DMA
+    return pl.pallas_call(
+        body,
+        out_shape=jax.ShapeDtypeStruct((length, width), BF16),
+        in_specs=[anywhere] * 16,
+        out_specs=vmem,
+        scratch_shapes=[
+            pltpu.VMEM(owners.shape[::-1], jnp.int32),
+            pltpu.VMEM(owners.shape[::-1], jnp.int32),
+            pltpu.VMEM((heads, length), F32),
+            pltpu.VMEM((heads, depth), BF16),
+            pltpu.VMEM((heads, depth), BF16),
+            pltpu.VMEM((heads, depth), BF16),
+            pltpu.VMEM((1, head_dim), F32),
+            pltpu.SMEM((heads,), F32),
+            pltpu.VMEM((length, 16), F32),
+            pltpu.VMEM((length, depth), BF16),
+            pltpu.VMEM((rows, depth), BF16),
+            pltpu.VMEM((6, depth, width), BF16),
+            pltpu.VMEM((2, pieces, piece_rows, half), BF16),
+            pltpu.VMEM((3, length, width), BF16),
+            pltpu.VMEM((store.shape[0], passage_rows, width), BF16),
+            pltpu.VMEM((store.shape[0], passage_rows, width), BF16),
+            pltpu.VMEM((store.shape[0], passage_rows, width), BF16),
+            pltpu.VMEM((devices, pieces, piece_rows, half), BF16),
+            pltpu.VMEM((devices, pieces, piece_rows, half), BF16),
+            pltpu.VMEM((devices, pieces, piece_blocks, lanes), F32),
+            pltpu.VMEM((devices, pieces, piece_rows, half), BF16),
+            pltpu.VMEM((devices, pieces, piece_blocks, lanes), F32),
+            pltpu.VMEM((3, 2, pieces, piece_rows, half), BF16),
+            pltpu.VMEM((3, 2, pieces, piece_blocks, lanes), F32),
+            pltpu.VMEM((length, width), F32),
+            pltpu.VMEM((2, length, 128), F32),
+            pltpu.VMEM((8, 128), jnp.int32),
+            pltpu.VMEM((devices, 8, 128), jnp.int32),
+            pltpu.SMEM((devices, 8, 128), jnp.int32),
+            dma((8 + pieces + 8,)),
+            dma,
+            dma((2,)),
+            dma((2, devices, pieces)),
+            dma((devices, pieces)),
+            dma((devices, pieces)),
+            dma((devices, pieces)),
+            dma((devices, pieces)),
+            dma((devices, pieces)),
+            dma((3, 2, pieces)),
+            dma((3, 2, pieces)),
+            dma((devices,)),
+            dma((devices,)),
+            dma((pieces,)),
+        ],
+        compiler_params=pltpu.CompilerParams(
+            collective_id=0, has_side_effects=True, vmem_limit_bytes=60 * 1024 * 1024
+        ),
+        cost_estimate=pl.CostEstimate(
+            flops=12_000_000_000, bytes_accessed=20_000_000, transcendentals=0
+        ),
+        name="whole",
+    )(
+        owners.T,
+        entries.T,
+        extra_forgetting_exponent.T,
+        strength_weight.T,
+        decay_weight.T,
+        retrieval_gate_weight.T,
+        output_norm_gain[None, :],
+        head_decay_rate,
+        tokens,
+        store.reshape(rows, depth),
+        *weights,
+    )
+
+
+def ring_attend(q_ref, named, me, sibling, kv_own, kv_sib, o_ref, stat_ref, passage_rows, head_dim):
+    length, half = q_ref.shape
+    heads = half // head_dim
+    blocks = length // BLOCK
+    scale = head_dim ** (-0.5)
+    nothing = jnp.zeros((BLOCK, head_dim), BF16)
+
+    def find(pairs, device):
+        hit = jnp.int32(0)
+        for owner, entry in pairs:
+            hit = hit + (owner == device).astype(jnp.int32) * (entry + 1)
+        found = jnp.minimum(hit, 1)
+        return hit - found, (1 - found).astype(F32) * MISSING
+
+    places, scores = [], []
+    for block in range(blocks):
+        pairs = named(block)
+        row_own, bias_own = find(pairs, me)
+        row_sib, bias_sib = find(pairs, sibling)
+        places.append((row_own, bias_own, row_sib, bias_sib))
+        query = q_ref[block * BLOCK : (block + 1) * BLOCK, :]
+        spread = jnp.concatenate(
+            [
+                jnp.concatenate(
+                    [
+                        query[:, head * head_dim : (head + 1) * head_dim] if head == place else nothing
+                        for place in range(heads)
+                    ],
+                    axis=1,
+                )
+                for head in range(heads)
+            ],
+            axis=0,
+        )
+        keys = jnp.concatenate(
+            [
+                kv_own[row_own, :, :half],
+                kv_sib[row_sib, :, :half],
+            ],
+            axis=0,
+        )
+        scores.append(dot_nt(keys, spread))
+    weights, stats = [], []
+    for block in range(blocks):
+        _, bias_own, _, bias_sib = places[block]
+        raw = scores[block]
+        own = raw[:passage_rows] * scale + bias_own
+        sib = raw[passage_rows:] * scale + bias_sib
+        peak = jnp.max(jnp.maximum(own, sib), axis=0, keepdims=True)
+        e_own = jnp.exp(own - peak)
+        e_sib = jnp.exp(sib - peak)
+        total = jnp.sum(e_own + e_sib, axis=0, keepdims=True)
+        inv = 1.0 / total
+        weights.append(jnp.concatenate([e_own * inv, e_sib * inv], axis=0).astype(BF16))
+        stats.append(peak + jnp.log(total))
+    for block in range(blocks):
+        row_own, _, row_sib, _ = places[block]
+        values = jnp.concatenate(
+            [
+                kv_own[row_own, :, half:],
+                kv_sib[row_sib, :, half:],
+            ],
+            axis=0,
+        )
+        result = dot_tn(weights[block], values)
+        for head in range(heads):
+            cols = slice(head * head_dim, (head + 1) * head_dim)
+            o_ref[block * BLOCK : (block + 1) * BLOCK, cols] = result[
+                head * BLOCK : (head + 1) * BLOCK, cols
+            ].astype(BF16)
+    rows = jnp.concatenate(stats, axis=0)
+    spare = stat_ref.shape[1] - rows.shape[1]
+    if spare:
+        rows = jnp.concatenate([rows, jnp.zeros((blocks, spare), F32)], axis=1)
+    stat_ref[...] = rows
+
+
+def ring_kernel(
     chips,
     head_dim,
     passage_rows,
@@ -461,7 +1276,7 @@
                 for place in range(per)
             ]
 
-        attend_unit(
+        ring_attend(
             qbuf.at[at],
             named,
             me,
@@ -607,7 +1422,7 @@
                 copy.wait_send()
 
 
-def per_device(
+def ring_device(
     chips,
     tokens,
     owners,
@@ -647,7 +1462,7 @@
     ]
 
     def body(owners_ref, entries_ref, extra_ref, s1, s2, s3, gain_ref, rate_ref, tok, sto, *rest):
-        whole_kernel(
+        ring_kernel(
             chips, head_dim, passage_rows, owners_ref, entries_ref, extra_ref, (s1, s2, s3),
             gain_ref, rate_ref, tok, sto, rest[:6], *rest[6:],
         )
@@ -694,7 +1509,7 @@
         cost_estimate=pl.CostEstimate(
             flops=12_000_000_000, bytes_accessed=20_000_000, transcendentals=0
         ),
-        name="whole",
+        name="ring",
     )(
         owners.T,
         entries.T,
@@ -712,8 +1527,9 @@
 
 def solution(mesh):
     rows = ("grp", "st")
+    chips = mesh.shape["st"] // 2
     return jax.shard_map(
-        functools.partial(per_device, mesh.shape["st"] // 2),
+        functools.partial(line_device if chips // 2 == 2 else ring_device, chips),
         mesh=mesh,
         in_specs=(
             P(rows, None),

time: 98.8 us -> 57.8 us (0.59)
  Pallas kernels: 96.8 us -> 55 us
    pallas_call x1, Pallas kernels: 96.8 us -> 55 us  [line_device(): pl.pallas_call(body, out_shape=jax.ShapeDtypeStruct((length, width), BF16...]
where the time goes in v1:
time: 57.8 us; the launch traced here: 56.8 us
  Pallas kernels  55 us (95%)
  local copies, waits for them, and re-layouts  1.87 us (3%)
    pallas_call x1, Pallas kernels, line_device(): pl.pallas_call(body, out_shape=jax.ShapeDtypeStruct((length, width), BF16...  55 us
    unnamed x1, local copies, waits for them, and re-layouts  1.87 us

profile of v1, /device:TPU:1, one launch (start us, length us, event | category | flops | bytes accessed | tf_op | source)
XLA Modules:
  0.0 56.8 jit_solution(12285174194066194683)
XLA Ops:
  0.0 55.0 %whole.1 = bf16[512,512]{1,0:T(8,128)(2,1)} custom-call(s32[4,8]{1,0:T(4,128)} %bitcast.13, s32[4,8]{1,0:T(4,128)} %bitcast.14, f32[4,512]{1,0:T(4,128)} %bitcast.12, bf16[4,2048]{1,0:T(4,128)(2,1)} %bitcast.9, bf16[4,2048]{1,0:T(4,128)(2,1)} %bitcast.10, bf16[4,2048]{1,0:T(4,128)(2,1)} %bitcast.11, f32[1,128]{1,0:T(1,128)} %bitcast.15, f32[4]{0:T(128)} %refs_7_.1, ...), custom_call_target="tpu_custom_call" | custom-call | flops 12000000000 | bytes 20000000 | tf_op jit(solution)/shard_map/whole/pallas_call | solution.py:924
  55.0 1.9 %copy.18 = bf16[512,512]{1,0:T(8,128)(2,1)} copy(bf16[512,512]{1,0:T(8,128)(2,1)} %whole.1) | data formatting | bytes 1048576

commit v2 on v1

--- a/solution.py
+++ b/solution.py
@@ -126,7 +126,7 @@
     which = lax.broadcasted_iota(jnp.int32, (heads, length), 0)
     rate = jnp.zeros((heads, length), F32)
     for head in range(heads):
-        rate = jnp.where(which == head, rate_ref[head], rate)
+        rate = jnp.where(which == head, rate_ref[:, head : head + 1], rate)
     decay = -rate * softplus + extra_ref[...]
     rgate = jax.nn.sigmoid(rows[2 * heads : 3 * heads])
     tri = jnp.where(
@@ -313,7 +313,6 @@
     recv_q,
     send_r,
     send_s,
-    recv_r,
     recv_s,
     recv_f,
     recv_g,
@@ -347,6 +346,35 @@
             device_id_type=pl.DeviceIdType.MESH,
         )
 
+    rq_w, pk_w, pv_w, q_w = 0, 1, 2, 3
+
+    def token_rows(piece):
+        at = pl.ds(piece * piece_rows, piece_rows)
+        return pltpu.make_async_copy(tokens_hbm.at[at], tok.at[at], load_sem.at[6 + piece])
+
+    def query_weight(which, index):
+        at = pl.ds(pl.multiple_of(which * half, half), half)
+        return pltpu.make_async_copy(
+            weights_hbm[rq_w].at[:, at], wts.at[rq_w, :, at], load_sem.at[index]
+        )
+
+    loads = [None, None]
+    loads += [
+        pltpu.make_async_copy(weights_hbm[i], wts.at[i], load_sem.at[min(1 + i, 4)])
+        for i in range(1, 6)
+    ]
+    loads.append(pltpu.make_async_copy(store_hbm, sto, load_sem.at[5]))
+    first_loads = [token_rows(0), query_weight(core, 0)]
+    second_loads = [token_rows(piece) for piece in range(1, pieces)] + [query_weight(other, 1)]
+    small_refs = (small_a, small_b, small_c)
+    lesser_loads = [
+        pltpu.make_async_copy(src, dst, load_sem.at[6 + pieces + i])
+        for i, (src, dst) in enumerate(
+            zip(lesser, (owners_ref, entries_ref, extra_ref) + small_refs + (gain_ref, rate_ref))
+        )
+    ]
+    for copy in first_loads + second_loads + lesser_loads[:2]:
+        copy.start()
     barrier = pltpu.get_barrier_semaphore()
 
     @pl.loop(1, devices)
@@ -358,42 +386,6 @@
             device_id_type=pl.DeviceIdType.MESH,
         )
 
-    rq_w, pk_w, pv_w, q_w = 0, 1, 2, 3
-
-    def token_rows(piece):
-        at = pl.ds(piece * piece_rows, piece_rows)
-        return pltpu.make_async_copy(tokens_hbm.at[at], tok.at[at], load_sem.at[8 + piece])
-
-    def query_weight(which, index):
-        at = pl.ds(pl.multiple_of(which * half, half), half)
-        return pltpu.make_async_copy(
-            weights_hbm[rq_w].at[:, at], wts.at[rq_w, :, at], load_sem.at[index]
-        )
-
-    loads = [None, None]
-    loads += [
-        pltpu.make_async_copy(weights_hbm[i], wts.at[i], load_sem.at[1 + i]) for i in range(1, 6)
-    ]
-    loads.append(pltpu.make_async_copy(store_hbm, sto, load_sem.at[7]))
-    first_loads = [token_rows(0), query_weight(core, 0)]
-    second_loads = [token_rows(piece) for piece in range(1, pieces)] + [query_weight(other, 1)]
-    small_refs = (small_a, small_b, small_c)
-    lesser_loads = [
-        pltpu.make_async_copy(src, dst, load_sem.at[8 + pieces + i])
-        for i, (src, dst) in enumerate(
-            zip(lesser, (owners_ref, entries_ref, extra_ref) + small_refs + (gain_ref, rate_ref))
-        )
-    ]
-    for copy in first_loads + lesser_loads[:2] + second_loads:
-        copy.start()
-    lesser_loads[0].wait()
-    lesser_loads[1].wait()
-
-    want_mine[...] = jnp.zeros_like(want_mine)
-    want_mine[:per, :blocks] = owners_ref[...]
-    want_mine[per : 2 * per, :blocks] = entries_ref[...]
-    want_all[me] = want_mine[...]
-
     with jax.named_scope("wait_tok"):
         for copy in first_loads:
             copy.wait()
@@ -405,12 +397,15 @@
         cols = pl.ds(pl.multiple_of(side * half, half), half)
         rq[side, piece] = dot_nn(tok[at, :], wts[rq_w, :, cols]).astype(BF16)
 
+    def all_of(shaped, sem):
+        return pltpu.make_async_copy(shaped, shaped, sem)
+
     def want_copy(off):
         return rcopy(
             want_mine,
             want_all.at[me],
-            send_w.at[off - 1],
-            recv_w.at[me],
+            send_w,
+            recv_w,
             lax.rem(me + off, devices),
         )
 
@@ -418,7 +413,7 @@
         return rcopy(
             rq.at[side, piece],
             qbuf.at[me, piece],
-            send_q.at[way, chip * 2 + side, piece],
+            send_q.at[way],
             recv_q.at[me, piece],
             there * 2 + side,
         )
@@ -427,7 +422,7 @@
         return rcopy(
             qbuf.at[source, piece],
             qbuf.at[source, piece],
-            send_q.at[way, source, piece],
+            send_q.at[way],
             recv_q.at[source, piece],
             there * 2 + core,
         )
@@ -437,8 +432,8 @@
 
     def result_to(source, piece, dst, dstat, rsem, gsem, target):
         return (
-            rcopy(obuf.at[source, piece], dst, send_r.at[source, piece], rsem, target),
-            rcopy(sbuf.at[source, piece], dstat, send_s.at[source, piece], gsem, target),
+            rcopy(obuf.at[source, piece], dst, send_r, rsem, target),
+            rcopy(sbuf.at[source, piece], dstat, send_s, gsem, target),
         )
 
     def pass_result(source, piece, there):
@@ -447,7 +442,7 @@
             piece,
             rbuf.at[source, piece],
             rstat.at[source, piece],
-            recv_r.at[source, piece],
+            recv_q.at[source, piece],
             recv_s.at[source, piece],
             there * 2 + core,
         )
@@ -488,7 +483,10 @@
         def named(block):
             at = piece * piece_blocks + block
             return [
-                (want_smem[source, place, at], want_smem[source, per + place, at])
+                (
+                    want_smem[source, 0, place * blocks + at],
+                    want_smem[source, 0, (per + place) * blocks + at],
+                )
                 for place in range(per)
             ]
 
@@ -545,19 +543,30 @@
         pl.semaphore_wait(barrier, devices - 1)
     with jax.named_scope("rq1"):
 
-        @pl.loop(1, devices)
-        def _(off):
-            want_copy(off).start()
-
         own_first(0)
+        lesser_loads[0].wait()
+        lesser_loads[1].wait()
+        named_rows = [
+            ref[place : place + 1, :] for ref in (owners_ref, entries_ref) for place in range(per)
+        ]
+        want = jnp.concatenate(
+            named_rows + [jnp.zeros((1, want_mine.shape[1] - 2 * per * blocks), jnp.int32)], axis=1
+        )
+        want_mine[...] = want
+        want_all[me] = want
         for copy in second_loads:
             copy.wait()
-        for copy in lesser_loads[2:]:
-            copy.start()
         loads[1 + pv_w].start()
         for piece in range(1, pieces):
             project_query(core, piece)
             own_first(piece)
+
+        @pl.loop(1, devices)
+        def _(off):
+            want_copy(off).start()
+
+        for copy in lesser_loads[2:]:
+            copy.start()
         for piece in range(pieces):
             project_query(other, piece)
 
@@ -568,7 +577,7 @@
 
     def sib_copy(piece):
         return rcopy(
-            rq.at[other, piece], qbuf.at[me, piece], send_h.at[piece], recv_q.at[me, piece], sibling
+            rq.at[other, piece], qbuf.at[me, piece], send_h, recv_q.at[me, piece], sibling
         )
 
     rows = sto.shape[0]
@@ -646,19 +655,14 @@
 
     with jax.named_scope("wants"):
 
-        @pl.loop(1, devices)
-        def _(off):
-            source = lax.rem(me + off, devices)
-            rcopy(want_mine, want_all.at[source], send_w.at[0], recv_w.at[source], source).wait_recv()
-
+        all_of(want_all.at[pl.ds(0, devices - 1)], recv_w).wait()
         fetch = pltpu.make_async_copy(want_all, want_smem, want_sem)
         fetch.start()
         fetch.wait()
         swap.wait()
-        for i in range(3):
-            loads[1 + q_w + i].wait()
         for copy in lesser_loads[2:]:
             copy.wait()
+        all_of(wts.at[pl.ds(q_w, 3)], load_sem.at[4]).wait()
 
     @pl.when(inner)
     def _():
@@ -839,38 +843,19 @@
         def _():
             finish_all((1 - far_side, 2))
 
-    @pl.loop(1, devices)
-    def _(off):
-        want_copy(off).wait_send()
-
-    @pl.loop(0, pieces)
-    def _(piece):
-        sib_copy(piece).wait_send()
-        for copy in give_result(sibling, piece, 2):
-            copy.wait_send()
-
-    @pl.loop(0, 2 * pieces)
-    def _(step):
-        piece, which = lax.rem(step, pieces), step // pieces
-
-        @pl.when(inner)
-        def _():
-            edge, peer, beyond = chip + near, chip + far, chip + 2 * far
-            own_query(edge, which, piece, 0).wait_send()
-            own_query(peer, which, piece, 1).wait_send()
-            pass_query(edge * 2 + which, piece, peer, 1).wait_send()
-            pass_query(peer * 2 + which, piece, edge, 0).wait_send()
-            pass_query(beyond * 2 + which, piece, edge, 0).wait_send()
-            for where in (edge, peer, beyond):
-                for copy in give_result(where * 2 + which, piece, 0):
-                    copy.wait_send()
-
-        @pl.when(end)
-        def _():
-            own_query(chip + far, which, piece, 1).wait_send()
-            for distance in range(1, chips):
-                for copy in give_result((chip + far * distance) * 2 + which, piece, 0):
-                    copy.wait_send()
+    all_of(want_all.at[pl.ds(0, devices - 1)], send_w).wait()
+    all_of(qbuf.at[0], send_h).wait()
+    all_of(obuf.at[pl.ds(0, devices - 1)], send_r).wait()
+    all_of(sbuf.at[pl.ds(0, devices - 1)], send_s).wait()
+
+    @pl.when(inner)
+    def _():
+        all_of(qbuf.at[pl.ds(0, 6)], send_q.at[0]).wait()
+        all_of(qbuf.at[pl.ds(0, 4)], send_q.at[1]).wait()
+
+    @pl.when(end)
+    def _():
+        all_of(qbuf.at[pl.ds(0, 2)], send_q.at[1]).wait()
 
 
 def line_device(
@@ -905,7 +890,7 @@
     piece_rows, piece_blocks = length // pieces, blocks // pieces
     lanes = 2 * BLOCK
     vmem = pl.BlockSpec(memory_space=pltpu.VMEM)
-    anywhere = pl.BlockSpec(memory_space=pl.ANY)
+    anywhere = pl.BlockSpec(memory_space=pltpu.HBM)
     weights = [
         retrieval_query_weight,
         passage_key_weight,
@@ -921,7 +906,7 @@
         )
 
     dma = pltpu.SemaphoreType.DMA
-    return pl.pallas_call(
+    call = pl.pallas_call(
         body,
         out_shape=jax.ShapeDtypeStruct((length, width), BF16),
         in_specs=[anywhere] * 16,
@@ -934,7 +919,7 @@
             pltpu.VMEM((heads, depth), BF16),
             pltpu.VMEM((heads, depth), BF16),
             pltpu.VMEM((1, head_dim), F32),
-            pltpu.SMEM((heads,), F32),
+            pltpu.VMEM((1, heads), F32),
             pltpu.VMEM((length, 16), F32),
             pltpu.VMEM((length, depth), BF16),
             pltpu.VMEM((rows, depth), BF16),
@@ -953,32 +938,32 @@
             pltpu.VMEM((3, 2, pieces, piece_blocks, lanes), F32),
             pltpu.VMEM((length, width), F32),
             pltpu.VMEM((2, length, 128), F32),
-            pltpu.VMEM((8, 128), jnp.int32),
-            pltpu.VMEM((devices, 8, 128), jnp.int32),
-            pltpu.SMEM((devices, 8, 128), jnp.int32),
-            dma((8 + pieces + 8,)),
+            pltpu.VMEM((1, 128), jnp.int32),
+            pltpu.VMEM((devices, 1, 128), jnp.int32),
+            pltpu.SMEM((devices, 1, 128), jnp.int32),
+            dma((6 + pieces + 8,)),
             dma,
             dma((2,)),
-            dma((2, devices, pieces)),
+            dma((2,)),
             dma((devices, pieces)),
-            dma((devices, pieces)),
-            dma((devices, pieces)),
-            dma((devices, pieces)),
+            dma,
+            dma,
             dma((devices, pieces)),
             dma((3, 2, pieces)),
             dma((3, 2, pieces)),
-            dma((devices,)),
-            dma((devices,)),
-            dma((pieces,)),
+            dma,
+            dma,
+            dma,
         ],
         compiler_params=pltpu.CompilerParams(
-            collective_id=0, has_side_effects=True, vmem_limit_bytes=60 * 1024 * 1024
+            collective_id=0, has_side_effects=True, vmem_limit_bytes=54000 * 1024
         ),
         cost_estimate=pl.CostEstimate(
             flops=12_000_000_000, bytes_accessed=20_000_000, transcendentals=0
         ),
         name="whole",
-    )(
+    )
+    operands = (
         owners.T,
         entries.T,
         extra_forgetting_exponent.T,
@@ -986,11 +971,12 @@
         decay_weight.T,
         retrieval_gate_weight.T,
         output_norm_gain[None, :],
-        head_decay_rate,
+        head_decay_rate[None, :],
         tokens,
         store.reshape(rows, depth),
         *weights,
     )
+    return call(*[pltpu.with_memory_space_constraint(array, pltpu.HBM) for array in operands])
 
 
 def ring_attend(q_ref, named, me, sibling, kv_own, kv_sib, o_ref, stat_ref, passage_rows, head_dim):
@@ -1471,7 +1457,7 @@
     return pl.pallas_call(
         body,
         out_shape=jax.ShapeDtypeStruct((length, width), BF16),
-        in_specs=[vmem] * 7 + [pl.BlockSpec(memory_space=pltpu.SMEM)] + [anywhere] * 8,
+        in_specs=[vmem] * 8 + [anywhere] * 8,
         out_specs=vmem,
         scratch_shapes=[
             pltpu.VMEM((length, depth), BF16),
@@ -1518,7 +1504,7 @@
         decay_weight.T,
         retrieval_gate_weight.T,
         output_norm_gain[None, :],
-        head_decay_rate,
+        head_decay_rate[None, :],
         tokens,
         store.reshape(rows, depth),
         *weights,

time: 57.8 us -> 54.9 us (0.950)
  Pallas kernels: 55 us -> 53.6 us
  local copies, waits for them, and re-layouts: 1.87 us -> 0.8 us
    pallas_call x1, Pallas kernels: 55 us -> 53.6 us  [line_device(): call(*[pltpu.with_memory_space_constraint(array, pltpu.HBM) for array in...]
    unnamed x1, local copies, waits for them, and re-layouts: 1.87 us -> 0.8 us
where the time goes in v2:
time: 54.9 us; the launch traced here: 54.4 us
  Pallas kernels  53.6 us (98%)
  local copies, waits for them, and re-layouts  0.8 us (1%)
    pallas_call x1, Pallas kernels, line_device(): call(*[pltpu.with_memory_space_constraint(array, pltpu.HBM) for array in...  53.6 us

profile of v2, /device:TPU:1, one launch (start us, length us, event | category | flops | bytes accessed | tf_op | source)
XLA Modules:
  0.0 54.4 jit_solution(16642304977228648048)
XLA Ops:
  0.0 53.6 %whole.1 = bf16[512,512]{1,0:T(8,128)(2,1)S(1)} custom-call(s32[4,8]{1,0:T(4,128)} %bitcast.14, s32[4,8]{1,0:T(4,128)} %bitcast.15, f32[4,512]{1,0:T(4,128)} %bitcast.13, bf16[4,2048]{1,0:T(4,128)(2,1)} %bitcast.10, bf16[4,2048]{1,0:T(4,128)(2,1)} %bitcast.11, bf16[4,2048]{1,0:T(4,128)(2,1)} %bitcast.12, f32[1,128]{1,0:T(1,128)} %bitcast.16, ...), custom_call_target="tpu_custom_call" | custom-call | flops 12000000000 | bytes 20000000 | tf_op jit(solution)/shard_map/whole/pallas_call | solution.py:979
  53.6 0.8 %copy.18 = bf16[512,512]{1,0:T(8,128)(2,1)} copy(bf16[512,512]{1,0:T(8,128)(2,1)S(1)} %whole.1) | data formatting | bytes 1048576

commit v3 on v2

--- a/solution.py
+++ b/solution.py
@@ -373,7 +373,7 @@
             zip(lesser, (owners_ref, entries_ref, extra_ref) + small_refs + (gain_ref, rate_ref))
         )
     ]
-    for copy in first_loads + second_loads + lesser_loads[:2]:
+    for copy in lesser_loads[:2] + first_loads + second_loads:
         copy.start()
     barrier = pltpu.get_barrier_semaphore()
 
@@ -385,6 +385,17 @@
             device_id={"st": lax.rem(me + off, devices)},
             device_id_type=pl.DeviceIdType.MESH,
         )
+
+    lesser_loads[0].wait()
+    lesser_loads[1].wait()
+    named_rows = [
+        ref[place : place + 1, :] for ref in (owners_ref, entries_ref) for place in range(per)
+    ]
+    want = jnp.concatenate(
+        named_rows + [jnp.zeros((1, want_mine.shape[1] - 2 * per * blocks), jnp.int32)], axis=1
+    )
+    want_mine[...] = want
+    want_all[me] = want
 
     with jax.named_scope("wait_tok"):
         for copy in first_loads:
@@ -543,28 +554,17 @@
         pl.semaphore_wait(barrier, devices - 1)
     with jax.named_scope("rq1"):
 
+        @pl.loop(1, devices)
+        def _(off):
+            want_copy(off).start()
+
         own_first(0)
-        lesser_loads[0].wait()
-        lesser_loads[1].wait()
-        named_rows = [
-            ref[place : place + 1, :] for ref in (owners_ref, entries_ref) for place in range(per)
-        ]
-        want = jnp.concatenate(
-            named_rows + [jnp.zeros((1, want_mine.shape[1] - 2 * per * blocks), jnp.int32)], axis=1
-        )
-        want_mine[...] = want
-        want_all[me] = want
         for copy in second_loads:
             copy.wait()
         loads[1 + pv_w].start()
         for piece in range(1, pieces):
             project_query(core, piece)
             own_first(piece)
-
-        @pl.loop(1, devices)
-        def _(off):
-            want_copy(off).start()
-
         for copy in lesser_loads[2:]:
             copy.start()
         for piece in range(pieces):
@@ -624,13 +624,18 @@
         for piece in range(pieces):
             sib_copy(piece).start()
 
-        @pl.loop(0, tiles)
-        def _(m):
-            project_store(core, pk_w, kv_own, 0, m)
-
+        project_store(core, pk_w, kv_own, 0, 0)
     with jax.named_scope("relay0"):
         relay_first(0)
     with jax.named_scope("kv2"):
+
+        @pl.loop(1, tiles)
+        def _(m):
+            project_store(core, pk_w, kv_own, 0, m)
+
+        all_of(want_all.at[pl.ds(0, devices - 1)], recv_w).wait()
+        fetch = pltpu.make_async_copy(want_all, want_smem, want_sem)
+        fetch.start()
 
         @pl.loop(0, tiles)
         def _(m):
@@ -655,9 +660,6 @@
 
     with jax.named_scope("wants"):
 
-        all_of(want_all.at[pl.ds(0, devices - 1)], recv_w).wait()
-        fetch = pltpu.make_async_copy(want_all, want_smem, want_sem)
-        fetch.start()
         fetch.wait()
         swap.wait()
         for copy in lesser_loads[2:]:
@@ -677,8 +679,6 @@
             def _(piece):
                 attend(job(at(edge, core), piece), job(at(peer, core), piece))
 
-        with jax.named_scope("in_here"):
-            attend_here()
         with jax.named_scope("in23"):
 
             @pl.loop(0, pieces)
@@ -705,7 +705,8 @@
                 attend(job(at(beyond, other), piece))
                 project_mixer(2 * pieces + piece)
 
-        project_gates()
+        with jax.named_scope("in_here"):
+            attend_here()
         with jax.named_scope("in67"):
 
             @pl.loop(0, pieces)
@@ -727,6 +728,7 @@
                 merge(at(edge, core), piece)
                 begin(give_result(at(edge, core), piece, near_side))
 
+        project_gates()
         with jax.named_scope("in1011"):
 
             @pl.loop(0, pieces)
@@ -771,19 +773,19 @@
 
         with jax.named_scope("end01"):
             handle(1, core, False)
-        with jax.named_scope("end_here"):
-            attend_here()
         with jax.named_scope("end23"):
             handle(2, core, True, fill_two)
         with jax.named_scope("end45"):
             handle(3, core, True, fill_one)
-        project_gates()
+        with jax.named_scope("end_here"):
+            attend_here()
         with jax.named_scope("end67"):
             handle(3, other, True)
         with jax.named_scope("end89"):
             handle(2, other, True)
         for piece in range(pieces):
             begin(give_result(at(1, core), piece, far_side))
+        project_gates()
         with jax.named_scope("end1011"):
             handle(1, other, True)
 

time: 54.9 us -> 53.9 us (0.982)
  Pallas kernels: 53.6 us -> 52.5 us
    pallas_call x1, Pallas kernels: 53.6 us -> 52.5 us  [line_device(): call(*[pltpu.with_memory_space_constraint(array, pltpu.HBM) for array in...]
where the time goes in v3:
time: 53.9 us; the launch traced here: 53.3 us
  Pallas kernels  52.5 us (97%)
  local copies, waits for them, and re-layouts  0.8 us (1%)
    pallas_call x1, Pallas kernels, line_device(): call(*[pltpu.with_memory_space_constraint(array, pltpu.HBM) for array in...  52.5 us

profile of v3, /device:TPU:1, one launch (start us, length us, event | category | flops | bytes accessed | tf_op | source)
XLA Modules:
  0.0 53.3 jit_solution(18320024919560623369)
XLA Ops:
  0.0 52.5 %whole.1 = bf16[512,512]{1,0:T(8,128)(2,1)S(1)} custom-call(s32[4,8]{1,0:T(4,128)} %bitcast.14, s32[4,8]{1,0:T(4,128)} %bitcast.15, f32[4,512]{1,0:T(4,128)} %bitcast.13, bf16[4,2048]{1,0:T(4,128)(2,1)} %bitcast.10, bf16[4,2048]{1,0:T(4,128)(2,1)} %bitcast.11, bf16[4,2048]{1,0:T(4,128)(2,1)} %bitcast.12, f32[1,128]{1,0:T(1,128)} %bitcast.16, ...), custom_call_target="tpu_custom_call" | custom-call | flops 12000000000 | bytes 20000000 | tf_op jit(solution)/shard_map/whole/pallas_call | solution.py:981
  52.5 0.8 %copy.18 = bf16[512,512]{1,0:T(8,128)(2,1)} copy(bf16[512,512]{1,0:T(8,128)(2,1)S(1)} %whole.1) | data formatting | bytes 1048576

commit v4 on v3

--- a/solution.py
+++ b/solution.py
@@ -373,8 +373,6 @@
             zip(lesser, (owners_ref, entries_ref, extra_ref) + small_refs + (gain_ref, rate_ref))
         )
     ]
-    for copy in lesser_loads[:2] + first_loads + second_loads:
-        copy.start()
     barrier = pltpu.get_barrier_semaphore()
 
     @pl.loop(1, devices)
@@ -386,6 +384,8 @@
             device_id_type=pl.DeviceIdType.MESH,
         )
 
+    for copy in lesser_loads[:2] + first_loads:
+        copy.start()
     lesser_loads[0].wait()
     lesser_loads[1].wait()
     named_rows = [
@@ -397,6 +397,8 @@
     want_mine[...] = want
     want_all[me] = want
 
+    for copy in second_loads:
+        copy.start()
     with jax.named_scope("wait_tok"):
         for copy in first_loads:
             copy.wait()
@@ -564,11 +566,12 @@
         loads[1 + pv_w].start()
         for piece in range(1, pieces):
             project_query(core, piece)
-            own_first(piece)
         for copy in lesser_loads[2:]:
             copy.start()
         for piece in range(pieces):
             project_query(other, piece)
+            if piece + 1 < pieces:
+                own_first(piece + 1)
 
     @pl.when(end)
     def _():

time: 53.9 us -> 53.9 us (level)
  no operation moved by 1% of the time
where the time goes in v4:
time: 53.9 us; the launch traced here: 53.3 us
  Pallas kernels  52.5 us (97%)
  local copies, waits for them, and re-layouts  0.8 us (1%)
    pallas_call x1, Pallas kernels, line_device(): call(*[pltpu.with_memory_space_constraint(array, pltpu.HBM) for array in...  52.5 us

profile of v4, /device:TPU:1, one launch (start us, length us, event | category | flops | bytes accessed | tf_op | source)
XLA Modules:
  0.0 53.3 jit_solution(17979447207511167487)
XLA Ops:
  0.0 52.5 %whole.1 = bf16[512,512]{1,0:T(8,128)(2,1)S(1)} custom-call(s32[4,8]{1,0:T(4,128)} %bitcast.14, s32[4,8]{1,0:T(4,128)} %bitcast.15, f32[4,512]{1,0:T(4,128)} %bitcast.13, bf16[4,2048]{1,0:T(4,128)(2,1)} %bitcast.10, bf16[4,2048]{1,0:T(4,128)(2,1)} %bitcast.11, bf16[4,2048]{1,0:T(4,128)(2,1)} %bitcast.12, f32[1,128]{1,0:T(1,128)} %bitcast.16, ...), custom_call_target="tpu_custom_call" | custom-call | flops 12000000000 | bytes 20000000 | tf_op jit(solution)/shard_map/whole/pallas_call | solution.py:984
  52.5 0.8 %copy.18 = bf16[512,512]{1,0:T(8,128)(2,1)} copy(bf16[512,512]{1,0:T(8,128)(2,1)S(1)} %whole.1) | data formatting | bytes 1048576
